TPU v7x, 32 devices: a whole 2x2x4 slice. The times are simulated.
32 devices in a mesh: sp: 4 (over z), tp: 4 (over y, x), dp: 2 (over core).
Axes of the slice: x: 2, y: 2, z: 4, core: 2. Of those that a mesh axis runs over, the one named last changes fastest.
Arguments:
- latent: bfloat16 [2, 3072, 2048], P('dp', ('sp', 'tp')), may hold values from -3 to 3
- cond: bfloat16 [2, 2048], P('dp', 'sp'), may hold values from -6 to 6
- cond_ctx: bfloat16 [2048], P('sp'), may hold values from -6 to 6
- context: bfloat16 [2, 512, 2048], P('dp', 'sp'), may hold values from -6 to 6
- norm_gain: bfloat16 [2048], replicated, may hold values from 0.099609375 to 1.8984375
- mod_shift: bfloat16 [2048, 2048], P('sp', 'tp'), may hold values from -0.125 to 0.125
- mod_scale: bfloat16 [2048, 2048], P('sp', 'tp'), may hold values from -0.125 to 0.125
- mod_gate: bfloat16 [2048, 2048], P('sp', 'tp'), may hold values from -0.125 to 0.125
- w_query: bfloat16 [2048, 1024], P(None, 'tp'), may hold values from -0.125 to 0.125
- w_key: bfloat16 [2048, 256], P(None, 'tp'), may hold values from -0.125 to 0.125
- w_value: bfloat16 [2048, 256], P(None, 'tp'), may hold values from -0.125 to 0.125
- q_gain: bfloat16 [64], replicated, may hold values from 1 to 5.5
- k_gain: bfloat16 [64], replicated, may hold values from 1 to 5.5
- ctx_lift: float32 [16], P('tp'), may hold values from 1 to 3
- w_out: bfloat16 [1024, 2048], replicated, may hold values from -1.5 to 1.5
Outputs:
- mixed: bfloat16 [2, 3072, 2048], P('dp', ('sp', 'tp'))
All inputs are finite; a program needn't handle non-finite values.
Results may differ from a plain program's by a relative error of at most 0.009.
The roundings to bfloat16 on the way count: a program that leaves them out, or rounds other values in their place, can miss the bound.
Values may be sent and summed in bfloat16 or wider, within the bound.
A program may use at most 64 MiB of HBM per device.

v0:
```python
import jax
import jax.numpy as jnp
from jax import lax
from jax.sharding import PartitionSpec as P

HD = 64
GRID_W = 128
EPS = 1e-06
THETA = 10000.0


def modulate(row_block, gain_vec, shift_rows, scale_rows):
    values = row_block.astype(jnp.float32)
    normed = (
        values
        * lax.rsqrt(jnp.mean(values * values, axis=-1, keepdims=True) + EPS)
        * gain_vec.astype(jnp.float32)
    )
    return (normed * (1.0 + scale_rows) + shift_rows).astype(jnp.bfloat16)


def head_norm(raw_proj, gain_vec):
    samples, tokens, width = raw_proj.shape
    pieces = raw_proj.reshape(samples, tokens, width // HD, HD)
    normed = (
        pieces
        * lax.rsqrt(jnp.mean(pieces * pieces, axis=-1, keepdims=True) + EPS)
        * gain_vec.astype(jnp.float32)
    )
    return normed.transpose(0, 2, 1, 3)


def rotate(vector, positions):
    pairs_count = vector.shape[-1] // 4
    grid_row = (positions // GRID_W).astype(jnp.float32)
    grid_col = (positions % GRID_W).astype(jnp.float32)
    inverse = THETA ** (-jnp.arange(pairs_count, dtype=jnp.float32) / pairs_count)
    angles = jnp.concatenate([grid_row[:, None] * inverse, grid_col[:, None] * inverse], axis=-1)
    cosine = jnp.cos(angles)
    sine_val = jnp.sin(angles)
    first_half = vector[..., 0::2]
    second_half = vector[..., 1::2]
    turned = jnp.stack(
        [
            first_half * cosine - second_half * sine_val,
            first_half * sine_val + second_half * cosine,
        ],
        axis=-1,
    )
    return turned.reshape(vector.shape)


def split_heads(rows):
    samples, tokens, width = rows.shape
    return rows.reshape(samples, tokens, width // HD, HD).transpose(0, 2, 1, 3)


def on_device(
    latent,
    cond,
    cond_ctx,
    context,
    norm_gain,
    mod_shift,
    mod_scale,
    mod_gate,
    w_query,
    w_key,
    w_value,
    q_gain,
    k_gain,
    ctx_lift,
    w_out,
):
    samples = latent.shape[0]
    active = jax.nn.silu(
        jnp.concatenate([cond, cond_ctx[None, :]], axis=0).astype(jnp.float32)
    ).astype(jnp.bfloat16)
    partial_mods = tuple(
        (
            jnp.dot(active, weight, preferred_element_type=jnp.float32)
            for weight in (mod_shift, mod_scale, mod_gate)
        )
    )
    summed = lax.psum(partial_mods, "sp")
    shift_rows, scale_rows, gate_rows = lax.all_gather(summed, "tp", axis=1, tiled=True)
    modulated = modulate(
        latent, norm_gain, shift_rows[:samples, None, :], scale_rows[:samples, None, :]
    )
    ctx_mod = modulate(context, norm_gain, shift_rows[samples], scale_rows[samples])
    q_width = w_query.shape[1]
    k_width = w_key.shape[1]
    w_joint = jnp.concatenate([w_query, w_key, w_value], axis=1)
    projected = jnp.einsum(
        "srd,dc->src",
        lax.all_gather(modulated, "tp", axis=1, tiled=True),
        w_joint,
        preferred_element_type=jnp.float32,
    )
    tokens = projected.shape[1]
    k_heads = k_width // HD
    group_size = q_width // k_width
    positions = lax.axis_index("sp") * tokens + jnp.arange(tokens, dtype=jnp.int32)
    queries = rotate(head_norm(projected[..., :q_width], q_gain), positions).astype(jnp.bfloat16)
    queries = queries.reshape(samples, k_heads, group_size, tokens, HD)
    key_rows = rotate(
        head_norm(projected[..., q_width : q_width + k_width], k_gain), positions
    ).astype(jnp.bfloat16)
    value_rows = split_heads(projected[..., q_width + k_width :].astype(jnp.bfloat16))
    ctx_proj = jnp.einsum(
        "srd,dc->src", ctx_mod, w_joint[:, q_width:], preferred_element_type=jnp.float32
    )
    ctx_keys = head_norm(ctx_proj[..., :k_width], k_gain).astype(jnp.bfloat16)
    ctx_values = split_heads(ctx_proj[..., k_width:].astype(jnp.bfloat16))
    lift_table = ctx_lift.reshape(1, k_heads, group_size, 1, 1)
    factor = HD ** (-0.5)

    def absorb(state_now, key_block, value_block, score_lift):
        best_old, weight_sum, accumulated = state_now
        scores = (
            jnp.einsum("skgtd,skrd->skgtr", queries, key_block, preferred_element_type=jnp.float32)
            * factor
            + score_lift
        )
        peak = jnp.maximum(best_old, jnp.max(scores, axis=-1))
        weights = jnp.exp(scores - peak[..., None])
        rescale = jnp.exp(best_old - peak)
        weight_sum = weight_sum * rescale + jnp.sum(weights, axis=-1)
        accumulated = accumulated * rescale[..., None] + jnp.einsum(
            "skgtr,skrd->skgtd",
            weights.astype(jnp.bfloat16),
            value_block,
            preferred_element_type=jnp.float32,
        )
        return (peak, weight_sum, accumulated)

    stat_shape = (samples, k_heads, group_size, tokens)
    state_now = (
        jnp.full(stat_shape, -1e30, jnp.float32),
        jnp.zeros(stat_shape, jnp.float32),
        jnp.zeros(stat_shape + (HD,), jnp.float32),
    )
    all_ctx_keys, all_ctx_values = (
        lax.all_gather(ctx_keys, "sp", axis=2, tiled=True),
        lax.all_gather(ctx_values, "sp", axis=2, tiled=True),
    )
    state_now = absorb(state_now, all_ctx_keys, all_ctx_values, lift_table)
    key_piece = lax.all_gather(key_rows, "sp", axis=2, tiled=True)
    value_piece = lax.all_gather(value_rows, "sp", axis=2, tiled=True)
    block_count = key_piece.shape[2] // tokens
    key_blocks = jnp.moveaxis(key_piece.reshape(samples, k_heads, block_count, tokens, HD), 2, 0)
    value_blocks = jnp.moveaxis(
        value_piece.reshape(samples, k_heads, block_count, tokens, HD), 2, 0
    )

    def step_block(carry, blocks):
        return (absorb(carry, blocks[0], blocks[1], 0.0), None)

    state_out, unused = lax.scan(step_block, state_now, (key_blocks, value_blocks))
    state_now = state_out
    best_old, weight_sum, accumulated = state_now
    attended = (accumulated / weight_sum[..., None]).astype(jnp.bfloat16)
    head_rows = attended.transpose(0, 3, 1, 2, 4).reshape(samples, tokens, q_width)
    projected_out = jnp.einsum(
        "srq,qd->srd",
        lax.all_to_all(head_rows, "tp", split_axis=1, concat_axis=2, tiled=True),
        w_out,
        preferred_element_type=jnp.float32,
    )
    return (latent.astype(jnp.float32) + gate_rows[:samples, None, :] * projected_out).astype(
        jnp.bfloat16
    )


def solution(mesh):
    placed = (
        P("dp", ("sp", "tp"), None),
        P("dp", "sp"),
        P("sp"),
        P("dp", "sp", None),
        P(),
        P("sp", "tp"),
        P("sp", "tp"),
        P("sp", "tp"),
        P(None, "tp"),
        P(None, "tp"),
        P(None, "tp"),
        P(),
        P(),
        P("tp"),
        P(),
    )
    return jax.shard_map(
        on_device,
        mesh=mesh,
        in_specs=placed,
        out_specs=P("dp", ("sp", "tp"), None),
        check_vma=False,
    )
```

profile of v0, /device:TPU:0, one launch (start us, length us, event | category | flops | bytes accessed | tf_op | source)
XLA Modules:
  0.0 190.3 jit_solution(14167755606228791362)
XLA Ops:
  8.4 1.2 fusion.96
  10.9 20.5 %all-reduce = (f32[2,512]{1,0:T(2,128)S(1)}, f32[2,512]{1,0:T(2,128)S(1)}, f32[2,512]{1,0:T(2,128)S(1)}) all-reduce(f32[2,512]{1,0:T(2,128)S(1)} %fusion.94, f32[2,512]{1,0:T(2,128)S(1)} %fusion.96, f32[2,512]{1,0:T(2,128)S(1)} %fusion.98), channel_id=1, replica_groups=mesh['sp'=4,'tp'=4,'dp'=2] {'sp'}, use_global_device_ids=true, to_apply=%region_3.4 | all-reduce | flops 3072 | bytes 24576 | tf_op jit(solution)/shard_map/psum | solution.py:85
  31.4 8.2 %all_gather.25 = f32[2,2048]{1,0:T(2,128)S(1)} all-gather(f32[2,512]{1,0:T(2,128)S(1)} %get-tuple-element.88), channel_id=1, replica_groups=mesh['sp'=4,'tp'=4,'dp'=2] {'tp'}, dimensions={1}, use_global_device_ids=true | all-gather | bytes 20480 | tf_op jit(solution)/shard_map/all_gather | solution.py:86
  39.6 8.2 %all_gather.26 = f32[2,2048]{1,0:T(2,128)S(1)} all-gather(f32[2,512]{1,0:T(2,128)S(1)} %get-tuple-element.87), channel_id=1, replica_groups=mesh['sp'=4,'tp'=4,'dp'=2] {'tp'}, dimensions={1}, use_global_device_ids=true | all-gather | bytes 20480 | tf_op jit(solution)/shard_map/all_gather | solution.py:86
  48.4 1.4 fusion.31
  49.8 2.4 %fusion.35 = bf16[1,192,2048]{2,1,0:T(8,128)(2,1)} fusion(bf16[1,192,2048]{2,1,0:T(8,128)(2,1)} %param.17, f32[2048]{0:T(1024)S(1)} %bitcast.173, f32[2048]{0:T(1024)S(1)} %bitcast.172, f32[2048]{0:T(1024)S(1)} %convert_element_type.119, f32[192]{0:T(256)S(1)} %add_rsqrt_fusion.2), kind=kLoop, calls=%fused_computation.39 | loop fusion | flops 2359296 | bytes 1598208 | tf_op jit(solution)/shard_map/convert_element_type | solution.py:19
  53.6 12.0 %all_gather.28 = bf16[1,1,512,64]{2,3,1,0:T(8,128)(2,1)S(1)} all-gather(bf16[1,1,128,64]{2,3,1,0:T(8,128)(2,1)S(1)} %fusion.77), channel_id=1, replica_groups=mesh['sp'=4,'tp'=4,'dp'=2] {'sp'}, dimensions={2}, use_global_device_ids=true | all-gather | bytes 81920 | tf_op jit(solution)/shard_map/all_gather | solution.py:144
  65.7 12.6 %all-gather = bf16[1,512,64]{1,2,0:T(8,128)(2,1)} all-gather(bf16[1,128,64]{1,2,0:T(8,128)(2,1)S(1)} %slice.80), channel_id=2, replica_groups=mesh['sp'=4,'tp'=4,'dp'=2] {'sp'}, dimensions={1}, use_global_device_ids=true | all-gather | bytes 81920 | tf_op jit(solution)/shard_map/all_gather | solution.py:145
  80.1 13.4 %all-gather.4.cloned.1.call-done = bf16[1,768,2048]{2,1,0:T(8,128)(2,1)} async-done(((bf16[1,192,2048]{2,1,0:T(8,128)(2,1)}), bf16[1,768,2048]{2,1,0:T(8,128)(2,1)}) %all-gather.4.cloned.1.call-update) | async-done | bytes 3145744 | tf_op jit(solution)/shard_map/all_gather | solution.py:96
  93.5 3.7 %fusion.41 = f32[1,768,384]{1,2,0:T(8,128)S(1)} fusion(bf16[2048,64]{1,0:T(8,128)(2,1)S(1)} %copy.47, bf16[2048,64]{1,0:T(8,128)(2,1)S(1)} %copy.46, bf16[2048,256]{1,0:T(8,128)(2,1)} %param.25, bf16[1,768,2048]{2,1,0:T(8,128)(2,1)} %all-gather.4.cloned.1.call-done), kind=kOutput, calls=%fused_computation.45 | convolution fusion | flops 1212678144 | bytes 5898240 | tf_op jit(solution)/shard_map/srd,dc->src/dot_general | solution.py:94
  101.3 14.6 %all_gather.30 = bf16[1,1,3072,64]{2,3,1,0:T(8,128)(2,1)S(1)} all-gather(bf16[1,1,768,64]{2,3,1,0:T(8,128)(2,1)S(1)} %convert_element_type.131), channel_id=1, replica_groups=mesh['sp'=4,'tp'=4,'dp'=2] {'sp'}, dimensions={2}, use_global_device_ids=true | all-gather | bytes 491520 | tf_op jit(solution)/shard_map/all_gather | solution.py:148
  117.0 2.6 %copy-done.1 = f32[4,768,512]{1,2,0:T(8,128)} copy-done((f32[4,768,512]{1,2,0:T(8,128)}, f32[4,768,512]{1,2,0:T(8,128)S(1)}, u32[]{:S(2)}) %copy-start.1) | copy-done | bytes 6291480
  119.6 1.3 fusion.23
  120.9 15.5 %all-gather.1 = bf16[1,3072,64]{1,2,0:T(8,128)(2,1)S(1)} all-gather(bf16[1,768,64]{1,2,0:T(8,128)(2,1)S(1)} %slice.79), channel_id=3, replica_groups=mesh['sp'=4,'tp'=4,'dp'=2] {'sp'}, dimensions={1}, use_global_device_ids=true | all-gather | bytes 491520 | tf_op jit(solution)/shard_map/all_gather | solution.py:149
  136.8 4.3 %fusion.49 = f32[1,1,4,768,64]{3,4,2,1,0:T(8,128)S(1)} fusion(f32[4,768,512]{1,2,0:T(8,128)} %copy-done.1, f32[4,768]{1,0:T(4,128)S(1)} %get-tuple-element.106, f32[4]{0:T(128)S(1)} %copy-done.7, f32[4,768]{1,0:T(4,128)S(1)} %get-tuple-element.104, bf16[1,512,64]{1,2,0:T(8,128)(2,1)S(1)} %copy-done.6), kind=kOutput, calls=%fused_computation.49 | convolution fusion | flops 207814656 | bytes 7168016 | tf_op jit(solution)/shard_map/skgtr,skrd->skgtd/dot_general | solution.py:129
  141.0 19.7 %while.14 = (s32[]{:T(128)}, f32[1,1,4,768]{3,2,1,0:T(4,128)S(1)}, f32[1,1,4,768]{3,2,1,0:T(4,128)S(1)}, f32[1,1,4,768,64]{3,4,2,1,0:T(8,128)S(1)}, bf16[4,1,1,7...) while((s32[]{:T(128)}, f32[1,1,4,768]{3,2,1,0:T(4,128)S(1)}, ...), condition=%wide.region_13.14_spmd, body=%wide.region_10.13_spmd.sunk | while | flops 623256576 | bytes 30670940 | solution.py:159
  141.1 1.4 bitcast_reduce_fusion.2
  142.5 1.9 fusion.116
  144.4 1.6 fusion.115
  146.0 1.4 bitcast_reduce_fusion.2
  147.4 1.9 fusion.116
  149.3 1.6 fusion.115
  150.9 1.4 bitcast_reduce_fusion.2
  152.4 1.9 fusion.116
  154.3 1.6 fusion.115
  155.9 1.4 bitcast_reduce_fusion.2
  157.3 1.9 fusion.116
  159.2 1.6 fusion.115
  162.0 3.0 %reduce.15 = bf16[768,256]{1,0:T(8,128)(2,1)S(1)} reduce(bf16[768,1,256]{2,1,0:T(2,128)(2,1)S(1)} %bitcast.162, bf16[]{:T(256)} %broadcast.433), dimensions={1}, to_apply=%bitcast.124.reduce_sub_computation | reduce | bytes 786434
  165.9 3.5 %all-to-all-start = ((bf16[4,2,24576]{2,1,0:T(2,128)(2,1)}), bf16[4,2,24576]{2,1,0:T(2,128)(2,1)S(1)}, u32[]{:S(2)}, u32[]{:S(2)}) async-start(bf16[4,2,24576]{2,1,0:T(2,128)(2,1)} %reshape.683), calls=%async_computation | async-start | bytes 786432 | tf_op jit(solution)/shard_map/all_to_all | solution.py:166
  169.4 9.1 %all_gather.24 = f32[2,2048]{1,0:T(2,128)S(1)} all-gather(f32[2,512]{1,0:T(2,128)S(1)} %get-tuple-element.89), channel_id=1, replica_groups=mesh['sp'=4,'tp'=4,'dp'=2] {'tp'}, dimensions={1}, use_global_device_ids=true | all-gather | bytes 20480 | tf_op jit(solution)/shard_map/all_gather | solution.py:86
  179.3 4.1 %fusion.30 = bf16[1,192,2048]{2,1,0:T(8,128)(2,1)} fusion(bf16[192,1024]{1,0:T(8,128)(2,1)S(1)} %bitcast.171, bf16[1024,2048]{1,0:T(8,128)(2,1)} %param.31, bf16[1,192,2048]{2,1,0:T(8,128)(2,1)S(1)} %copy-done.2, f32[2048]{0:T(1024)S(1)} %bitcast.174), kind=kOutput, calls=%fused_computation.32 | convolution fusion | flops 806879232 | bytes 6168576 | tf_op jit(solution)/shard_map/srq,qd->srd/dot_general | solution.py:164
  (92 shorter events, 15.4 us)
Async XLA Ops:
  6.5 1.0 copy-start
  6.5 45.7 %copy-start.5 = (bf16[2048,64]{0,1:T(8,128)(2,1)S(1)}, bf16[2048,64]{0,1:T(8,128)(2,1)}, u32[]{:S(2)}) copy-start(bf16[2048,64]{0,1:T(8,128)(2,1)} %param.26) | copy-start | bytes 786436
  6.5 46.0 %copy-start.4 = (bf16[2048,64]{0,1:T(8,128)(2,1)S(1)}, bf16[2048,64]{0,1:T(8,128)(2,1)}, u32[]{:S(2)}) copy-start(bf16[2048,64]{0,1:T(8,128)(2,1)} %param.27) | copy-start | bytes 786436
  6.5 46.3 %copy-start.8 = (bf16[64]{0:T(256)(128)(2,1)S(1)}, bf16[64]{0:T(256)(128)(2,1)}, u32[]{:S(2)}) copy-start(bf16[64]{0:T(256)(128)(2,1)} %param.29) | copy-start | bytes 388
  6.5 46.3 %copy-start.9 = (bf16[64]{0:T(256)(128)(2,1)S(1)}, bf16[64]{0:T(256)(128)(2,1)}, u32[]{:S(2)}) copy-start(bf16[64]{0:T(256)(128)(2,1)} %param.28) | copy-start | bytes 388
  6.5 46.3 %copy-start.3 = (bf16[1,128,2048]{2,1,0:T(8,128)(2,1)S(1)}, bf16[1,128,2048]{2,1,0:T(8,128)(2,1)}, u32[]{:S(2)}) copy-start(bf16[1,128,2048]{2,1,0:T(8,128)(2,1)} %param.20) | copy-start | bytes 1572868
  6.6 86.9 %all-gather.4.cloned.1.call-start = ((), (), s32[]{:S(2)}) async-start(), calls=%async_computation.1 | async-start | bytes 3932160 | tf_op jit(solution)/shard_map/all_gather | solution.py:96
  97.5 18.4 %copy-start.7 = (f32[4]{0:T(128)S(1)}, f32[4]{0:T(128)}, u32[]{:S(2)}) copy-start(f32[4]{0:T(128)} %param.30) | copy-start | bytes 52
  116.9 2.7 %copy-start.1 = (f32[4,768,512]{1,2,0:T(8,128)}, f32[4,768,512]{1,2,0:T(8,128)S(1)}, u32[]{:S(2)}) copy-start(f32[4,768,512]{1,2,0:T(8,128)S(1)} %get-tuple-element.114) | copy-start | bytes 18874372
  117.0 19.8 %copy-start.6 = (bf16[1,512,64]{1,2,0:T(8,128)(2,1)S(1)}, bf16[1,512,64]{1,2,0:T(8,128)(2,1)}, u32[]{:S(2)}) copy-start(bf16[1,512,64]{1,2,0:T(8,128)(2,1)} %all-gather) | copy-start | bytes 196612
  160.8 18.5 %copy-start.2 = (bf16[1,192,2048]{2,1,0:T(8,128)(2,1)S(1)}, bf16[1,192,2048]{2,1,0:T(8,128)(2,1)}, u32[]{:S(2)}) copy-start(bf16[1,192,2048]{2,1,0:T(8,128)(2,1)} %param.17) | copy-start | bytes 2359300
  165.9 12.5 %all-to-all-start = ((bf16[4,2,24576]{2,1,0:T(2,128)(2,1)}), bf16[4,2,24576]{2,1,0:T(2,128)(2,1)S(1)}, u32[]{:S(2)}, u32[]{:S(2)}) async-start(bf16[4,2,24576]{2,1,0:T(2,128)(2,1)} %reshape.683), calls=%async_computation | async-start | bytes 786432 | tf_op jit(solution)/shard_map/all_to_all | solution.py:166
Sparse Core Ops, SparseCore 0:
  52.3 41.0 all-gather.3
where the time goes:
time: 191 us; the launch traced here: 190 us
  blocking collectives  101 us (53%)
  matrix products  30 us (16%)
  other arithmetic  20 us (10%)
  between operations  13.8 us (7%)
  waiting for transfers between devices  13.4 us (7%)
  local copies, waits for them, and re-layouts  8.75 us (5%)
  starting transfers between devices  3.5 us (2%)
    all_gather x3, blocking collectives, on_device(): lax.all_gather(summed, 'tp', axis=1, tiled=True)  25.4 us
    psum x1, blocking collectives, on_device(): summed = lax.psum(partial_mods, 'sp')  20.5 us
    all_gather x1, blocking collectives, on_device(): value_piece = lax.all_gather(value_rows, 'sp', axis=2, tiled=True)  15.5 us
    all_gather x1, blocking collectives, on_device(): key_piece = lax.all_gather(key_rows, 'sp', axis=2, tiled=True)  14.6 us
    all_gather x1, waiting for transfers between devices, on_device(): lax.all_gather(modulated, 'tp', axis=1, tiled=True)  13.4 us
    all_gather x1, blocking collectives, on_device(): lax.all_gather(ctx_values, 'sp', axis=2, tiled=True)  12.6 us
    all_gather x1, blocking collectives, on_device(): lax.all_gather(ctx_keys, 'sp', axis=2, tiled=True)  12 us
    dot_general x5, matrix products, absorb(): jnp.einsum('skgtr,skrd->skgtd', weights.astype(jnp.bfloat16), value_block...  11.7 us
  transfers between devices with their start and end apart: 2, of which 1 were waited for; matrix products, arithmetic and copies ran while one was open for 2% of the time, Pallas kernels for 0%

commit v1 on v0

--- a/solution.py
+++ b/solution.py
@@ -72,6 +72,20 @@
     ctx_lift,
     w_out,
 ):
+
+    def define_grid_now(x_local, net_axis):
+        nd = jax.lax.axis_size(net_axis)
+        found = [(dd, (dd + 1) % nd) for dd in range(nd)]
+
+        def leaves_show(now):
+            if len(now) == nd:
+                return now
+            return leaves_show([jax.lax.ppermute(now[0], perm=found, axis_name=net_axis), *now])
+
+        taken_in = leaves_show([x_local])
+        w2 = jnp.concatenate(taken_in, 2)
+        return jnp.roll(w2, (jax.lax.axis_index(net_axis) + 1) * x_local.shape[2], axis=2)
+
     samples = latent.shape[0]
     active = jax.nn.silu(
         jnp.concatenate([cond, cond_ctx[None, :]], axis=0).astype(jnp.float32)
@@ -146,7 +160,7 @@
     )
     state_now = absorb(state_now, all_ctx_keys, all_ctx_values, lift_table)
     key_piece = lax.all_gather(key_rows, "sp", axis=2, tiled=True)
-    value_piece = lax.all_gather(value_rows, "sp", axis=2, tiled=True)
+    value_piece = define_grid_now(value_rows, net_axis="sp")
     block_count = key_piece.shape[2] // tokens
     key_blocks = jnp.moveaxis(key_piece.reshape(samples, k_heads, block_count, tokens, HD), 2, 0)
     value_blocks = jnp.moveaxis(

time: 191 us -> 180 us (0.942)
  blocking collectives: 101 us -> 86.2 us
  starting transfers between devices: 3.5 us -> 6.58 us
  waiting for transfers between devices: 13.4 us -> 16.2 us
    all_gather x1 -> x0, blocking collectives: 15.5 us -> none  [on_device(): value_piece = lax.all_gather(value_rows, 'sp', axis=2, tiled=True)]
    ppermute x0 -> x3, waiting for transfers between devices: none -> 3.94 us  [leaves_show(): jax.lax.ppermute(now[0], perm=found, axis_name=net_axis)]
    ppermute x0 -> x3, starting transfers between devices: none -> 3.08 us  [leaves_show(): jax.lax.ppermute(now[0], perm=found, axis_name=net_axis)]
    dot_general x5, matrix products: 11.7 us -> 8.94 us  [absorb(): jnp.einsum('skgtr,skrd->skgtd', weights.astype(jnp.bfloat16), value_block...]
    unnamed x27 -> x38, local copies, waits for them, and re-layouts: 5.28 us -> 2.74 us
  transfers between devices with their start and end apart: 2 -> 5, of which waited for: 1 -> 2; matrix products, arithmetic and copies ran while one was open for 2% -> 7% of each run, Pallas kernels for 0% -> 0%
where the time goes in v1:
time: 180 us
  blocking collectives  86.2 us (48%)
  matrix products  28.1 us (16%)
  other arithmetic  21.1 us (12%)
  waiting for transfers between devices  16.2 us (9%)
  between operations  13.9 us (8%)
  local copies, waits for them, and re-layouts  7.38 us (4%)
  starting transfers between devices  6.58 us (4%)
    all_gather x3, blocking collectives, on_device(): lax.all_gather(summed, 'tp', axis=1, tiled=True)  25.4 us
    psum x1, blocking collectives, on_device(): summed = lax.psum(partial_mods, 'sp')  20.5 us
    all_gather x1, blocking collectives, on_device(): key_piece = lax.all_gather(key_rows, 'sp', axis=2, tiled=True)  15.1 us
    all_gather x1, blocking collectives, on_device(): lax.all_gather(ctx_keys, 'sp', axis=2, tiled=True)  12.6 us
    all_gather x1, blocking collectives, on_device(): lax.all_gather(ctx_values, 'sp', axis=2, tiled=True)  12.6 us
    all_gather x1, waiting for transfers between devices, on_device(): lax.all_gather(modulated, 'tp', axis=1, tiled=True)  12.3 us
    dot_general x5, matrix products, absorb(): jnp.einsum('skgtr,skrd->skgtd', weights.astype(jnp.bfloat16), value_block...  8.94 us
    dot_general x5, matrix products, absorb(): jnp.einsum('skgtd,skrd->skgtr', queries, key_block, preferred_element_typ...  7.6 us
  transfers between devices with their start and end apart: 5, of which 2 were waited for; matrix products, arithmetic and copies ran while one was open for 7% of the time, Pallas kernels for 0%

profile of v1, /device:TPU:0, one launch (start us, length us, event | category | flops | bytes accessed | tf_op | source)
XLA Modules:
  0.0 179.6 jit_solution(9768121297032490954)
XLA Ops:
  10.9 20.5 %all-reduce = (f32[2,512]{1,0:T(2,128)S(1)}, f32[2,512]{1,0:T(2,128)S(1)}, f32[2,512]{1,0:T(2,128)S(1)}) all-reduce(f32[2,512]{1,0:T(2,128)S(1)} %fusion.95, f32[2,512]{1,0:T(2,128)S(1)} %fusion.97, f32[2,512]{1,0:T(2,128)S(1)} %fusion.99), channel_id=1, replica_groups=mesh['sp'=4,'tp'=4,'dp'=2] {'sp'}, use_global_device_ids=true, to_apply=%region_3.4 | all-reduce | flops 3072 | bytes 24576 | tf_op jit(solution)/shard_map/psum | solution.py:99
  31.4 8.2 %all_gather.22 = f32[2,2048]{1,0:T(2,128)S(1)} all-gather(f32[2,512]{1,0:T(2,128)S(1)} %get-tuple-element.81), channel_id=1, replica_groups=mesh['sp'=4,'tp'=4,'dp'=2] {'tp'}, dimensions={1}, use_global_device_ids=true | all-gather | bytes 20480 | tf_op jit(solution)/shard_map/all_gather | solution.py:100
  39.6 8.2 %all_gather.23 = f32[2,2048]{1,0:T(2,128)S(1)} all-gather(f32[2,512]{1,0:T(2,128)S(1)} %get-tuple-element.80), channel_id=1, replica_groups=mesh['sp'=4,'tp'=4,'dp'=2] {'tp'}, dimensions={1}, use_global_device_ids=true | all-gather | bytes 20480 | tf_op jit(solution)/shard_map/all_gather | solution.py:100
  48.4 1.4 fusion.31
  49.8 2.4 %fusion.35 = bf16[1,192,2048]{2,1,0:T(8,128)(2,1)} fusion(bf16[1,192,2048]{2,1,0:T(8,128)(2,1)} %param.17, f32[2048]{0:T(1024)S(1)} %bitcast.183, f32[2048]{0:T(1024)S(1)} %bitcast.182, f32[2048]{0:T(1024)S(1)} %convert_element_type.119, f32[192]{0:T(256)S(1)} %add_rsqrt_fusion.2), kind=kLoop, calls=%fused_computation.39 | loop fusion | flops 2359296 | bytes 1598208 | tf_op jit(solution)/shard_map/convert_element_type | solution.py:19
  54.1 12.6 %all_gather.25 = bf16[1,1,512,64]{2,3,1,0:T(8,128)(2,1)} all-gather(bf16[1,1,128,64]{2,3,1,0:T(8,128)(2,1)S(1)} %fusion.78), channel_id=1, replica_groups=mesh['sp'=4,'tp'=4,'dp'=2] {'sp'}, dimensions={2}, use_global_device_ids=true | all-gather | bytes 81920 | tf_op jit(solution)/shard_map/all_gather | solution.py:158
  66.8 12.6 %all-gather = bf16[1,512,64]{1,2,0:T(8,128)(2,1)} all-gather(bf16[1,128,64]{1,2,0:T(8,128)(2,1)S(1)} %slice.81), channel_id=2, replica_groups=mesh['sp'=4,'tp'=4,'dp'=2] {'sp'}, dimensions={1}, use_global_device_ids=true | all-gather | bytes 81920 | tf_op jit(solution)/shard_map/all_gather | solution.py:159
  81.2 12.3 %all-gather.3.cloned.1.call-done = bf16[1,768,2048]{2,1,0:T(8,128)(2,1)} async-done(((bf16[1,192,2048]{2,1,0:T(8,128)(2,1)}), bf16[1,768,2048]{2,1,0:T(8,128)(2,1)}) %all-gather.3.cloned.1.call-update) | async-done | bytes 3145744 | tf_op jit(solution)/shard_map/all_gather | solution.py:110
  93.5 3.7 %fusion.41 = f32[1,768,384]{1,2,0:T(8,128)S(1)} fusion(bf16[2048,64]{1,0:T(8,128)(2,1)S(1)} %copy.46, bf16[2048,64]{1,0:T(8,128)(2,1)S(1)} %copy.45, bf16[2048,256]{1,0:T(8,128)(2,1)} %param.25, bf16[1,768,2048]{2,1,0:T(8,128)(2,1)} %all-gather.3.cloned.1.call-done), kind=kOutput, calls=%fused_computation.45 | convolution fusion | flops 1212678144 | bytes 5898240 | tf_op jit(solution)/shard_map/srd,dc->src/dot_general | solution.py:108
  99.3 1.5 collective-permute-start
  102.5 1.9 %fusion.21 = (f32[4,768]{1,0:T(4,128)S(1)}, f32[4,768,512]{1,2,0:T(8,128)S(1)}) fusion(f32[4]{0:T(128)S(1)} %copy-done.8, bf16[4,768,64]{1,2,0:T(8,128)(2,1)S(1)} %convert_element_type.125, bf16[1,1,512,64]{2,3,1,0:T(8,128)(2,1)} %all_gather.25), kind=kOutput, calls=%fused_computation.23 | convolution fusion | flops 206042112 | bytes 6762512 | tf_op jit(solution)/shard_map/skgtd,skrd->skgtr/dot_general | solution.py:135
  105.8 1.5 fusion.49
  108.5 1.5 collective-permute-start.1
  111.0 3.9 %collective-permute-done.1 = bf16[1,1,768,64]{2,3,1,0:T(8,128)(2,1)S(1)} collective-permute-done((bf16[1,1,768,64]{2,3,1,0:T(8,128)(2,1)S(1)}, bf16[1,1,768,64]{2,3,1,0:T(8,128)(2,1)S(1)}, u32[]{:S(2)}, u32[]{:S(2)}) %collective-permute-start.1) | collective-permute-done | bytes 98336 | tf_op jit(solution)/shard_map/ppermute | solution.py:83
  114.9 15.1 %all_gather.27 = bf16[1,1,3072,64]{2,3,1,0:T(8,128)(2,1)S(1)} all-gather(bf16[1,1,768,64]{2,3,1,0:T(8,128)(2,1)S(1)} %convert_element_type.131), channel_id=1, replica_groups=mesh['sp'=4,'tp'=4,'dp'=2] {'sp'}, dimensions={2}, use_global_device_ids=true | all-gather | bytes 491520 | tf_op jit(solution)/shard_map/all_gather | solution.py:162
  130.4 19.7 %while.14 = (s32[]{:T(128)}, f32[1,1,4,768]{3,2,1,0:T(4,128)S(1)}, f32[1,1,4,768]{3,2,1,0:T(4,128)S(1)}, f32[1,1,4,768,64]{3,4,2,1,0:T(8,128)S(1)}, bf16[4,1,1,7...) while((s32[]{:T(128)}, f32[1,1,4,768]{3,2,1,0:T(4,128)S(1)}, ...), condition=%wide.region_13.14_spmd, body=%wide.region_10.13_spmd.sunk | while | flops 623256576 | bytes 30670940 | solution.py:173
  130.4 1.4 bitcast_reduce_fusion.2
  131.9 1.9 %fusion.117 = f32[1,1,4,768,64]{3,4,2,1,0:T(8,128)S(1)} fusion(f32[768,4,768]{2,0,1:T(8,128)S(1)} %get-tuple-element.159, f32[4,768]{1,0:T(4,128)S(1)} %bitcast.168, f32[1,1,4,768,64]{3,4,2,1,0:T(8,128)S(1)} %get-tuple-element.172, f32[4,768]{1,0:T(4,128)S(1)} %get-tuple-element.160, bf16[4,1,1,768,64]{3,4,2,1,0:T(8,128)(2,1)S(1)} %get-tuple-element.183, ...), kind=kOutput, calls=%fused_computation.7.clone.1 | convolution fusion | flops 309460992 | bytes 11132932 | tf_op jit(solution)/shard_map/while/body/eval_jaxpr/skgtr,skrd->skgtd/dot_general | solution.py:143
  133.8 1.6 fusion.116
  135.4 1.4 bitcast_reduce_fusion.2
  136.8 1.9 %fusion.117 = f32[1,1,4,768,64]{3,4,2,1,0:T(8,128)S(1)} fusion(f32[768,4,768]{2,0,1:T(8,128)S(1)} %get-tuple-element.159, f32[4,768]{1,0:T(4,128)S(1)} %bitcast.168, f32[1,1,4,768,64]{3,4,2,1,0:T(8,128)S(1)} %get-tuple-element.172, f32[4,768]{1,0:T(4,128)S(1)} %get-tuple-element.160, bf16[4,1,1,768,64]{3,4,2,1,0:T(8,128)(2,1)S(1)} %get-tuple-element.183, ...), kind=kOutput, calls=%fused_computation.7.clone.1 | convolution fusion | flops 309460992 | bytes 11132932 | tf_op jit(solution)/shard_map/while/body/eval_jaxpr/skgtr,skrd->skgtd/dot_general | solution.py:143
  138.7 1.6 fusion.116
  140.3 1.4 bitcast_reduce_fusion.2
  141.8 1.9 %fusion.117 = f32[1,1,4,768,64]{3,4,2,1,0:T(8,128)S(1)} fusion(f32[768,4,768]{2,0,1:T(8,128)S(1)} %get-tuple-element.159, f32[4,768]{1,0:T(4,128)S(1)} %bitcast.168, f32[1,1,4,768,64]{3,4,2,1,0:T(8,128)S(1)} %get-tuple-element.172, f32[4,768]{1,0:T(4,128)S(1)} %get-tuple-element.160, bf16[4,1,1,768,64]{3,4,2,1,0:T(8,128)(2,1)S(1)} %get-tuple-element.183, ...), kind=kOutput, calls=%fused_computation.7.clone.1 | convolution fusion | flops 309460992 | bytes 11132932 | tf_op jit(solution)/shard_map/while/body/eval_jaxpr/skgtr,skrd->skgtd/dot_general | solution.py:143
  143.6 1.6 fusion.116
  145.2 1.4 bitcast_reduce_fusion.2
  146.7 1.9 %fusion.117 = f32[1,1,4,768,64]{3,4,2,1,0:T(8,128)S(1)} fusion(f32[768,4,768]{2,0,1:T(8,128)S(1)} %get-tuple-element.159, f32[4,768]{1,0:T(4,128)S(1)} %bitcast.168, f32[1,1,4,768,64]{3,4,2,1,0:T(8,128)S(1)} %get-tuple-element.172, f32[4,768]{1,0:T(4,128)S(1)} %get-tuple-element.160, bf16[4,1,1,768,64]{3,4,2,1,0:T(8,128)(2,1)S(1)} %get-tuple-element.183, ...), kind=kOutput, calls=%fused_computation.7.clone.1 | convolution fusion | flops 309460992 | bytes 11132932 | tf_op jit(solution)/shard_map/while/body/eval_jaxpr/skgtr,skrd->skgtd/dot_general | solution.py:143
  148.6 1.6 fusion.116
  151.4 3.0 %reduce.15 = bf16[768,256]{1,0:T(8,128)(2,1)S(1)} reduce(bf16[768,1,256]{2,1,0:T(2,128)(2,1)S(1)} %bitcast.170, bf16[]{:T(256)} %broadcast.437), dimensions={1}, to_apply=%bitcast.127.reduce_sub_computation | reduce | bytes 786434
  155.3 3.5 %all-to-all-start = ((bf16[4,2,24576]{2,1,0:T(2,128)(2,1)}), bf16[4,2,24576]{2,1,0:T(2,128)(2,1)S(1)}, u32[]{:S(2)}, u32[]{:S(2)}) async-start(bf16[4,2,24576]{2,1,0:T(2,128)(2,1)} %reshape.681), calls=%async_computation | async-start | bytes 786432 | tf_op jit(solution)/shard_map/all_to_all | solution.py:180
  158.7 9.1 %all_gather.21 = f32[2,2048]{1,0:T(2,128)S(1)} all-gather(f32[2,512]{1,0:T(2,128)S(1)} %get-tuple-element.82), channel_id=1, replica_groups=mesh['sp'=4,'tp'=4,'dp'=2] {'tp'}, dimensions={1}, use_global_device_ids=true | all-gather | bytes 20480 | tf_op jit(solution)/shard_map/all_gather | solution.py:100
  168.7 4.1 %fusion.30 = bf16[1,192,2048]{2,1,0:T(8,128)(2,1)} fusion(bf16[192,1024]{1,0:T(8,128)(2,1)S(1)} %bitcast.181, bf16[1024,2048]{1,0:T(8,128)(2,1)} %param.31, bf16[1,192,2048]{2,1,0:T(8,128)(2,1)S(1)} %copy-done.1, f32[2048]{0:T(1024)S(1)} %bitcast.184), kind=kOutput, calls=%fused_computation.32 | convolution fusion | flops 806879232 | bytes 6168576 | tf_op jit(solution)/shard_map/srq,qd->srd/dot_general | solution.py:178
  (109 shorter events, 19.3 us)
Async XLA Ops:
  6.5 1.0 copy-start
  6.5 45.7 %copy-start.5 = (bf16[2048,64]{0,1:T(8,128)(2,1)S(1)}, bf16[2048,64]{0,1:T(8,128)(2,1)}, u32[]{:S(2)}) copy-start(bf16[2048,64]{0,1:T(8,128)(2,1)} %param.26) | copy-start | bytes 786436
  6.5 46.0 %copy-start.4 = (bf16[2048,64]{0,1:T(8,128)(2,1)S(1)}, bf16[2048,64]{0,1:T(8,128)(2,1)}, u32[]{:S(2)}) copy-start(bf16[2048,64]{0,1:T(8,128)(2,1)} %param.27) | copy-start | bytes 786436
  6.5 46.3 %copy-start.10 = (bf16[64]{0:T(256)(128)(2,1)S(1)}, bf16[64]{0:T(256)(128)(2,1)}, u32[]{:S(2)}) copy-start(bf16[64]{0:T(256)(128)(2,1)} %param.29) | copy-start | bytes 388
  6.5 46.3 %copy-start.11 = (bf16[64]{0:T(256)(128)(2,1)S(1)}, bf16[64]{0:T(256)(128)(2,1)}, u32[]{:S(2)}) copy-start(bf16[64]{0:T(256)(128)(2,1)} %param.28) | copy-start | bytes 388
  6.5 46.8 %copy-start.2 = (bf16[1,128,2048]{2,1,0:T(8,128)(2,1)S(1)}, bf16[1,128,2048]{2,1,0:T(8,128)(2,1)}, u32[]{:S(2)}) copy-start(bf16[1,128,2048]{2,1,0:T(8,128)(2,1)} %param.20) | copy-start | bytes 1572868
  6.6 86.9 %all-gather.3.cloned.1.call-start = ((), (), s32[]{:S(2)}) async-start(), calls=%async_computation.1 | async-start | bytes 3932160 | tf_op jit(solution)/shard_map/all_gather | solution.py:110
  81.2 17.6 %copy-start.9 = (f32[64]{0:T(128)S(1)}, f32[64]{0:T(128)}, u32[]{:S(2)}) copy-start(f32[64]{0:T(128)} %convert_element_type.121) | copy-start | bytes 772
  98.7 3.9 %copy-start.8 = (f32[4]{0:T(128)S(1)}, f32[4]{0:T(128)}, u32[]{:S(2)}) copy-start(f32[4]{0:T(128)} %param.30) | copy-start | bytes 52
  99.3 9.1 %collective-permute-start = (bf16[1,1,768,64]{2,3,1,0:T(8,128)(2,1)}, bf16[1,1,768,64]{2,3,1,0:T(8,128)(2,1)S(1)}, u32[]{:S(2)}, u32[]{:S(2)}) collective-permute-start(bf16[1,1,768,64]{2,3,1,0:T(8,128)(2,1)} %fusion.67), channel_id=1, source_target_pairs={{0,8},{8,16},{16,24},{24,0},{1,9},{9,17},{17,25},{25,1},{2,10},{10... | collective-permute-start | bytes 294920 | tf_op jit(solution)/shard_map/ppermute | solution.py:83
  104.4 1.4 copy-start.7
  105.8 1.5 copy-start.3
  105.8 1.5 copy-start.6
  108.5 6.5 %collective-permute-start.1 = (bf16[1,1,768,64]{2,3,1,0:T(8,128)(2,1)S(1)}, bf16[1,1,768,64]{2,3,1,0:T(8,128)(2,1)S(1)}, u32[]{:S(2)}, u32[]{:S(2)}) collective-permute-start(bf16[1,1,768,64]{2,3,1,0:T(8,128)(2,1)S(1)} %collective-permute-done), channel_id=1, source_target_pairs={{0,8},{8,16},{16,24},{24,0},{1,9},{9,17},{17,25},{25,1},{2,10},{10... | collective-permute-start | bytes 294920 | tf_op jit(solution)/shard_map/ppermute | solution.py:83
  114.9 15.1 %collective-permute-start.2 = (bf16[1,1,768,64]{2,3,1,0:T(8,128)(2,1)S(1)}, bf16[1,1,768,64]{2,3,1,0:T(8,128)(2,1)S(1)}, u32[]{:S(2)}, u32[]{:S(2)}) collective-permute-start(bf16[1,1,768,64]{2,3,1,0:T(8,128)(2,1)S(1)} %collective-permute-done.1), channel_id=1, source_target_pairs={{0,8},{8,16},{16,24},{24,0},{1,9},{9,17},{17,25},{25,1},{2,10},{10... | collective-permute-start | bytes 294920 | tf_op jit(solution)/shard_map/ppermute | solution.py:83
  150.3 18.4 %copy-start.1 = (bf16[1,192,2048]{2,1,0:T(8,128)(2,1)S(1)}, bf16[1,192,2048]{2,1,0:T(8,128)(2,1)}, u32[]{:S(2)}) copy-start(bf16[1,192,2048]{2,1,0:T(8,128)(2,1)} %param.17) | copy-start | bytes 2359300
  155.3 12.5 %all-to-all-start = ((bf16[4,2,24576]{2,1,0:T(2,128)(2,1)}), bf16[4,2,24576]{2,1,0:T(2,128)(2,1)S(1)}, u32[]{:S(2)}, u32[]{:S(2)}) async-start(bf16[4,2,24576]{2,1,0:T(2,128)(2,1)} %reshape.681), calls=%async_computation | async-start | bytes 786432 | tf_op jit(solution)/shard_map/all_to_all | solution.py:180
Sparse Core Ops, SparseCore 0:
  52.3 41.0 all-gather.2
